TPU v7x, 256 devices: a whole 4x4x8 slice. The times are simulated.
256 devices in a mesh: sp: 32 (over z, x), tp: 8 (over y, core).
Axes of the slice: x: 4, y: 4, z: 8, core: 2. Of those that a mesh axis runs over, the one named last changes fastest.
Arguments:
- tokens: bfloat16 [2, 6144, 4096], P(None, 'sp', 'tp'), may hold values from -12 to 12
- query_weight: bfloat16 [4096, 2048], P(None, 'tp'), may hold values from -0.09375 to 0.09375
- key_weight: bfloat16 [4096, 2048], P(None, 'tp'), may hold values from -0.09375 to 0.09375
- value_weight: bfloat16 [4096, 2048], P(None, 'tp'), may hold values from -0.09375 to 0.09375
- gate_weight: bfloat16 [4096, 2048], P(None, 'tp'), may hold values from -0.09375 to 0.09375
- beta_weight: bfloat16 [4096, 16], P(None, 'tp'), may hold values from -0.09375 to 0.09375
- decay_weight: bfloat16 [4096, 16], P(None, 'tp'), may hold values from -0.09375 to 0.09375
- beta_bias: float32 [16], P('tp'), may hold values from -6 to -3
- rate_log: float32 [16], P('tp'), may hold values from -12 to -2.5
- out_gain: float32 [128], replicated, may hold values from 0.1 to 1.9
- new_query: bfloat16 [2, 16, 128], P(None, 'tp'), may hold values from -6 to 6
- new_key: bfloat16 [2, 16, 128], P(None, 'tp'), may hold values from -6 to 6
- new_value: bfloat16 [2, 16, 128], P(None, 'tp'), may hold values from -6 to 6
- new_beta: float32 [2, 16], P(None, 'tp'), may hold values from 0.1 to 0.9
- new_decay: float32 [2, 16], P(None, 'tp'), may hold values from 0.3 to 1
Outputs:
- mixed_out: bfloat16 [2, 6144, 2048], P(None, 'sp', 'tp')
- cache: bfloat16 [2, 16, 128, 128], P(None, 'tp', 'sp')
- first_out: float32 [2, 2048], P(None, 'tp')
All inputs are finite; a program needn't handle non-finite values.
Results may differ from a plain program's by a relative error of at most 0.0073.
Values may be sent and summed in bfloat16 or wider, within the bound.
No kernel may reach another device: no remote copies, remote signals or barrier semaphores. Data moves between devices by JAX's collectives and lax.ppermute only.
A program may use at most 64 MiB of HBM per device.

v0:
```python
import jax
import jax.numpy as jnp
from jax import lax
from jax.sharding import Mesh
from jax.sharding import PartitionSpec as P

BLOCK = 64
SP = ("sp_0", "sp_1")
unit_floor = 1.0
norm_floor = 0.001
highest = lax.Precision.HIGHEST


def neutral_like(value, identity):
    return jax.tree.map(
        lambda a, e: jnp.broadcast_to(jnp.asarray(e, a.dtype), a.shape), value, identity
    )


def carried_in(value, axes, combine, identity):
    before = start = neutral_like(value, identity)
    subtotal = value
    for axis in reversed(axes):
        length, index = (lax.axis_size(axis), lax.axis_index(axis))
        pieces = jax.tree.map(lambda part: lax.all_gather(part, axis), subtotal)
        inside, subtotal = (start, start)
        for k in range(length):
            passed = k < index
            subtotal = combine(subtotal, jax.tree.map(lambda part: part[k], pieces))
            inside = jax.tree.map(lambda new, old: jnp.where(passed, new, old), subtotal, inside)
        before = combine(inside, before)
    return before


def split_up(value, dim, length):
    before, after = (value.shape[:dim], value.shape[dim + 1 :])
    return jnp.moveaxis(value.reshape(*before, length, -1, *after), dim, 0)


def summed_on_arrival(value, axis, dim):
    parts = split_up(value, dim, lax.axis_size(axis))
    arrived = lax.all_to_all(parts, axis, split_axis=0, concat_axis=0, tiled=True)
    return arrived.astype(jnp.float32).sum(axis=0)


def copy_for_each(value, axis):
    length = lax.axis_size(axis)
    return lax.all_to_all(
        jnp.broadcast_to(value[None], (length, *value.shape)), axis, 0, 0, tiled=True
    )


def over_copies(value, axis):
    everything = copy_for_each(value, axis)
    return jnp.sum(everything, axis=0)


def in_one(arrays, axis):
    ravelled, at, gathered = (jnp.concatenate([a.reshape(-1) for a in arrays]), 0, [])
    subtotal = over_copies(ravelled, axis)
    for a in arrays:
        gathered.append(subtotal[at : at + a.size].reshape(a.shape))
        at += a.size
    return tuple(gathered)


def matmul(form, left, right):
    return jnp.einsum(form, left, right, precision=highest)


def unit_rows(values):
    return values * lax.rsqrt(jnp.sum(values * values, axis=-1, keepdims=True) + unit_floor)


def head_norm(values, out_gain):
    return (
        values
        * lax.rsqrt(jnp.mean(values * values, axis=-1, keepdims=True) + norm_floor)
        * out_gain
    )


def stored(values):
    return lax.optimization_barrier(values.astype(jnp.bfloat16)).astype(jnp.float32)


def unit_lower_inverse(lower_part):
    extent = lower_part.shape[-1]
    nilpotent = -lower_part
    inverse = jnp.eye(extent, dtype=jnp.float32) + nilpotent
    for _ in range(extent.bit_length() - 2):
        nilpotent = matmul("...ij,...jk->...ik", nilpotent, nilpotent)
        inverse = inverse + matmul("...ij,...jk->...ik", nilpotent, inverse)
    return inverse


def prepare(
    query_rows,
    key_rows,
    value_rows,
    beta_in,
    decay_in,
    beta_bias,
    rate_log,
    seq_count,
    length,
    head_count,
):
    extent = query_rows.shape[-1] // head_count
    blocks = length // BLOCK

    def by_head(values):
        shaped = values.reshape(seq_count, blocks, BLOCK, head_count, extent)
        return shaped.transpose(0, 3, 1, 2, 4).reshape(
            seq_count * head_count, blocks, BLOCK, extent
        )

    def by_scalar(values):
        shaped = values.reshape(seq_count, blocks, BLOCK, head_count)
        return shaped.transpose(0, 3, 1, 2).reshape(seq_count * head_count, blocks, BLOCK)

    queries = unit_rows(by_head(query_rows))
    key_unit = unit_rows(by_head(key_rows))
    values = by_head(value_rows)
    strength = by_scalar(jax.nn.sigmoid(beta_in + beta_bias))
    decays = by_scalar(-jnp.exp(rate_log) * jax.nn.softplus(decay_in))
    return (queries, key_unit, values, strength, decays)


def block_terms(queries, key_unit, values, strength, decays):
    extent = decays.shape[-1]
    cumulative = jnp.cumsum(decays, axis=-1)
    causal = jnp.tril(jnp.ones((extent, extent), bool))
    strict = jnp.tril(jnp.ones((extent, extent), bool), -1)
    spread = cumulative[..., :, None] - cumulative[..., None, :]
    weights = jnp.where(causal, jnp.exp(jnp.where(causal, spread, 0.0)), 0.0)
    key_beta = key_unit * strength[..., None]
    lower_part = jnp.where(strict, matmul("...td,...sd->...ts", key_beta, key_unit) * weights, 0.0)
    inverse = unit_lower_inverse(lower_part)
    update = matmul("...ts,...se->...te", inverse, values * strength[..., None])
    carry_w = matmul("...ts,...sd->...td", inverse, key_beta * jnp.exp(cumulative)[..., None])
    scores = matmul("...td,...sd->...ts", queries, key_unit) * weights
    query_decay = queries * jnp.exp(cumulative)[..., None]
    last_log = cumulative[..., -1]
    key_decay = key_unit * jnp.exp(last_log[..., None] - cumulative)[..., None]
    return (update, carry_w, query_decay, scores, key_decay, last_log)


def finish_read(recall, retrieve, query_unit, key_unit, new_value, new_beta, new_decay, out_gain):
    seq_count, head_count, extent = recall.shape
    intersect = jnp.sum(key_unit * query_unit, axis=-1)
    fresh_values = new_value.astype(jnp.float32) - new_decay[..., None] * retrieve
    read_heads = new_decay[..., None] * recall + (new_beta * intersect)[..., None] * fresh_values
    return head_norm(read_heads, out_gain).reshape(seq_count, head_count * extent)


def project_rows(shard_rows, weights):
    row_count = shard_rows.shape[-1]
    flat_rows = shard_rows.reshape(-1, row_count)
    return tuple(
        (jnp.dot(flat_rows, weight, preferred_element_type=jnp.float32) for weight in weights)
    )


def shards(
    tokens,
    query_weight,
    key_weight,
    value_weight,
    gate_weight,
    beta_weight,
    decay_weight,
    beta_bias,
    rate_log,
    out_gain,
    new_query,
    new_key,
    new_value,
    new_beta,
    new_decay,
):
    seq_count, span_len, _ = tokens.shape
    head_count = rate_log.shape[0]
    weights = (query_weight, key_weight, value_weight, gate_weight, beta_weight, decay_weight)
    totals = project_rows(lax.all_gather(tokens, "tp", axis=2, tiled=True), weights)
    query_rows = stored(totals[0])
    key_rows = stored(totals[1])
    value_rows = stored(totals[2])
    gate_rows = stored(totals[3])
    prepared = prepare(
        query_rows,
        key_rows,
        value_rows,
        totals[4],
        totals[5],
        beta_bias,
        rate_log,
        seq_count,
        span_len,
        head_count,
    )
    block_data = block_terms(*prepared)
    batch_size = block_data[0].shape[0]
    extent = block_data[0].shape[-1]
    identity = jnp.broadcast_to(jnp.eye(extent, dtype=jnp.float32), (batch_size, extent, extent))

    def advance(carried, inputs):
        state_now, reach_map = carried
        u_block, w_block, qg_block, score_block, kd_block, gl_block = inputs
        fresh_values = u_block - matmul("btd,bde->bte", w_block, state_now)
        block_out = matmul("btd,bde->bte", qg_block, state_now) + matmul(
            "bts,bse->bte", score_block, fresh_values
        )
        reach_rows = qg_block - matmul("bts,bsd->btd", score_block, w_block)
        factor = jnp.exp(gl_block)[:, None, None]
        transit = factor * identity - matmul("bsd,bse->bde", kd_block, w_block)
        state_next = state_now * factor + matmul("bsd,bse->bde", kd_block, fresh_values)
        map_next = matmul("bde,bef->bdf", transit, reach_map)
        return ((state_next, map_next), (block_out, matmul("btd,bde->bte", reach_rows, reach_map)))

    inputs = tuple((jnp.moveaxis(member, 1, 0) for member in block_data))
    start_state = jnp.zeros((batch_size, extent, extent), jnp.float32)
    (local_state, local_map), (local_out, reach_all) = lax.scan(
        advance, (start_state, identity), inputs
    )

    def compose(earlier, later):
        return (
            matmul("bde,bef->bdf", later[0], earlier[0]),
            matmul("bde,bef->bdf", later[0], earlier[1]) + later[1],
        )

    prefix = carried_in(
        (local_map, local_state), SP, compose, (identity, jnp.zeros_like(local_state))
    )
    incoming = prefix[1]
    block_total = local_out + matmul("nbtd,bde->nbte", reach_all, incoming)
    blocks = span_len // BLOCK
    heads_out = block_total.reshape(blocks, seq_count, head_count, BLOCK, extent).transpose(
        1, 0, 3, 2, 4
    )
    heads_out = heads_out.reshape(seq_count, span_len, head_count, extent)
    gate_values = gate_rows.reshape(seq_count, span_len, head_count, extent)
    mixed_out = (head_norm(heads_out, out_gain) * jax.nn.silu(gate_values)).astype(jnp.bfloat16)
    mixed_out = mixed_out.reshape(seq_count, span_len, head_count * extent)
    final_state = matmul("bde,bef->bdf", local_map, incoming) + local_state
    final_cast = final_state.reshape(seq_count, head_count, extent, extent).astype(jnp.bfloat16)
    row_count = extent // lax.axis_size(SP)
    row_start = lax.axis_index(SP) * row_count
    query_unit = unit_rows(new_query.astype(jnp.float32))
    key_unit = unit_rows(new_key.astype(jnp.float32))
    is_last = lax.axis_index(SP) == lax.axis_size(SP) - 1
    own_term = jnp.where(is_last, final_cast.astype(jnp.float32), 0.0)
    cache_rows = summed_on_arrival(own_term.astype(jnp.bfloat16), SP, 2).astype(jnp.bfloat16)
    memory = lax.optimization_barrier(cache_rows).astype(jnp.float32)
    query_part = lax.dynamic_slice_in_dim(query_unit, row_start, row_count, 2)
    key_part = lax.dynamic_slice_in_dim(key_unit, row_start, row_count, 2)
    recall, retrieve = in_one(
        (matmul("shde,shd->she", memory, query_part), matmul("shde,shd->she", memory, key_part)), SP
    )
    first_out = finish_read(
        recall, retrieve, query_unit, key_unit, new_value, new_beta, new_decay, out_gain
    )
    return (mixed_out, cache_rows, first_out)


def solution(mesh):
    torus = Mesh(mesh.devices.reshape(8, 4, mesh.shape["tp"]), ("sp_0", "sp_1", "tp"))
    in_specs = (
        P(None, SP, "tp"),
        P(None, "tp"),
        P(None, "tp"),
        P(None, "tp"),
        P(None, "tp"),
        P(None, "tp"),
        P(None, "tp"),
        P("tp"),
        P("tp"),
        P(),
        P(None, "tp", None),
        P(None, "tp", None),
        P(None, "tp", None),
        P(None, "tp"),
        P(None, "tp"),
    )
    out_specs = (P(None, SP, "tp"), P(None, "tp", SP, None), P(None, "tp"))
    return jax.shard_map(
        shards, mesh=torus, in_specs=in_specs, out_specs=out_specs, check_vma=False
    )
```

profile of v0, /device:TPU:8, one launch (start us, length us, event | category | flops | bytes accessed | tf_op | source)
XLA Modules:
  0.0 295.3 jit_solution(3390538268324986770)
XLA Ops:
  9.4 32.6 %all-gather.10.cloned.1.call-done = bf16[2,192,4096]{2,1,0:T(8,128)(2,1)} async-done(((bf16[2,192,512]{2,1,0:T(8,128)(2,1)}), bf16[2,192,4096]{2,1,0:T(8,128)(2,1)}) %all-gather.10.cloned.1.call-update) | async-done | bytes 3145744 | tf_op jit(solution)/shard_map/all_gather | solution.py:185
  42.0 2.8 fusion.91
  46.8 2.9 convolution_convert_fusion.1
  51.3 2.8 fusion.50
  54.3 3.5 %convolution_convert_fusion.3 = bf16[384,256]{1,0:T(8,128)(2,1)S(1)} fusion(bf16[384,4096]{1,0:T(8,128)(2,1)} %bitcast.236, bf16[4096,256]{1,0:T(8,128)(2,1)} %param.19), kind=kOutput, calls=%fused_computation.61 | convolution fusion | flops 805404672 | bytes 5439488 | tf_op jit(solution)/shard_map/dot_general | solution.py:161
  59.4 3.6 %convolution_convert_fusion.2 = bf16[384,256]{1,0:T(8,128)(2,1)S(1)} fusion(bf16[384,4096]{1,0:T(8,128)(2,1)} %bitcast.237, bf16[4096,256]{1,0:T(8,128)(2,1)} %param.20), kind=kOutput, calls=%fused_computation.60 | convolution fusion | flops 805404672 | bytes 5439488 | tf_op jit(solution)/shard_map/dot_general | solution.py:161
  73.8 1.5 fusion.39
  75.3 29.5 %while.17 = (s32[]{:T(128)}, f32[4,128,128]{2,1,0:T(8,128)S(1)}, f32[4,128,128]{2,1,0:T(8,128)S(1)}, f32[3,4,64,128]{3,2,0,1:T(8,128)}, f32[3,4,64,128]{3,2,0,1:...) while((s32[]{:T(128)}, f32[4,128,128]{2,1,0:T(8,128)S(1)}, ...), condition=%wide.region_4.5_spmd.clone, body=%wide.region_3.4_spmd.clone.sunk | while | flops 403210240 | bytes 5445847 | solution.py:223
  79.5 1.5 convolution_add_fusion.23
  83.2 1.5 convolution_subtract_fusion.7
  89.3 1.5 convolution_add_fusion.23
  99.2 1.5 convolution_add_fusion.23
  106.4 26.9 %all-gather.12.cloned.1.call-done = f32[16,128,128]{2,1,0:T(8,128)} async-done(((f32[4,128,128]{2,1,0:T(8,128)}), f32[16,128,128]{2,1,0:T(8,128)}) %all-gather.12.cloned.1.call-update) | async-done | bytes 1048592 | tf_op jit(solution)/shard_map/all_gather | solution.py:25
  139.8 22.4 %all-gather.16.cloned.1.call-done = f32[16,128,128]{2,1,0:T(8,128)} async-done(((f32[4,128,128]{2,1,0:T(8,128)}), f32[16,128,128]{2,1,0:T(8,128)}) %all-gather.16.cloned.1.call-update) | async-done | bytes 1048592 | tf_op jit(solution)/shard_map/all_gather | solution.py:25
  168.5 4.3 %convolution_convert_fusion = bf16[384,256]{1,0:T(8,128)(2,1)} fusion(bf16[384,4096]{1,0:T(8,128)(2,1)} %bitcast.238, bf16[4096,256]{1,0:T(8,128)(2,1)} %param.21), kind=kOutput, calls=%fused_computation.58 | convolution fusion | flops 805404672 | bytes 5439488 | tf_op jit(solution)/shard_map/dot_general | solution.py:161
  173.9 31.2 %all-gather.14.cloned.1.call-done = f32[32,128,128]{2,1,0:T(8,128)} async-done(((f32[4,128,128]{2,1,0:T(8,128)}), f32[32,128,128]{2,1,0:T(8,128)}) %all-gather.14.cloned.1.call-update) | async-done | bytes 2097168 | tf_op jit(solution)/shard_map/all_gather | solution.py:25
  205.1 41.1 %all-gather.18.cloned.1.call-done = f32[32,128,128]{2,1,0:T(8,128)} async-done(((f32[4,128,128]{2,1,0:T(8,128)}), f32[32,128,128]{2,1,0:T(8,128)}) %all-gather.18.cloned.1.call-update) | async-done | bytes 2097168 | tf_op jit(solution)/shard_map/all_gather | solution.py:25
  246.2 1.5 convolution_add_fusion.20
  254.7 7.1 %all-to-all-start = ((bf16[32,2,2,4,128]{4,3,2,1,0:T(4,128)(2,1)}), bf16[32,2,2,4,128]{4,3,2,1,0:T(4,128)(2,1)S(1)}, u32[]{:S(2)}, u32[]{:S(2)}) async-start(bf16[32,2,2,4,128]{4,3,2,1,0:T(4,128)(2,1)} %bitcast.193), calls=%async_computation | async-start | bytes 262144 | tf_op jit(solution)/shard_map/all_to_all | solution.py:42
  261.8 1.6 fusion.38
  265.2 7.1 %all-to-all-done = bf16[32,2,2,4,128]{4,3,2,1,0:T(4,128)(2,1)S(1)} async-done(((bf16[32,2,2,4,128]{4,3,2,1,0:T(4,128)(2,1)}), bf16[32,2,2,4,128]{4,3,2,1,0:T(4,128)(2,1)S(1)}, u32[]{:S(2)}, u32[]{:S(2)}) %all-to-all-start) | async-done | bytes 131104 | tf_op jit(solution)/shard_map/all_to_all | solution.py:42
  273.4 3.8 %all-to-all-start.1 = ((f32[32,1,1024]{2,1,0:T(1,128)}), f32[32,1,1024]{2,1,0:T(1,128)S(1)}, u32[]{:S(2)}, u32[]{:S(2)}) async-start(f32[32,1,1024]{2,1,0:T(1,128)} %broadcast_in_dim.80), calls=%async_computation.1 | async-start | bytes 262144 | tf_op jit(solution)/shard_map/all_to_all | solution.py:48
  277.3 1.7 fusion.60
  279.0 8.8 %all-to-all-done.1 = f32[32,1,1024]{2,1,0:T(1,128)S(1)} async-done(((f32[32,1,1024]{2,1,0:T(1,128)}), f32[32,1,1024]{2,1,0:T(1,128)S(1)}, u32[]{:S(2)}, u32[]{:S(2)}) %all-to-all-start.1) | async-done | bytes 131104 | tf_op jit(solution)/shard_map/all_to_all | solution.py:48
  (195 shorter events, 67.1 us)
Async XLA Ops:
  7.2 39.7 %copy-start = (bf16[4096,256]{1,0:T(8,128)(2,1)S(1)}, bf16[4096,256]{1,0:T(8,128)(2,1)}, u32[]{:S(2)}) copy-start(bf16[4096,256]{1,0:T(8,128)(2,1)} %param.18) | copy-start | bytes 6291460
  7.2 34.8 %all-gather.10.cloned.1.call-start = ((), (), s32[]{:S(2)}) async-start(), calls=%async_computation.2 | async-start | bytes 3538944 | tf_op jit(solution)/shard_map/all_gather | solution.py:185
  7.9 125.4 %all-gather.12.cloned.1.call-start = ((), (), s32[]{:S(2)}) async-start(), calls=%async_computation.3 | async-start | bytes 1310720 | tf_op jit(solution)/shard_map/all_gather | solution.py:25
  59.4 3.8 %copy-start.20 = (f32[2,2,3,64,128]{4,3,1,0,2:T(8,128)S(1)}, f32[2,2,3,64,128]{4,3,1,0,2:T(8,128)}, u32[]{:S(2)}) copy-start(f32[2,2,3,64,128]{4,3,1,0,2:T(8,128)} %copy.189) | copy-start | bytes 1179652
  105.6 56.6 %all-gather.16.cloned.1.call-start = ((), (), s32[]{:S(2)}) async-start(), calls=%async_computation.5 | async-start | bytes 1310720 | tf_op jit(solution)/shard_map/all_gather | solution.py:25
  106.3 98.8 %all-gather.14.cloned.1.call-start = ((), (), s32[]{:S(2)}) async-start(), calls=%async_computation.4 | async-start | bytes 2359296 | tf_op jit(solution)/shard_map/all_gather | solution.py:25
  133.3 4.2 %copy-start.3 = (f32[16,128,128]{2,1,0:T(8,128)S(1)}, f32[16,128,128]{2,1,0:T(8,128)}, u32[]{:S(2)}) copy-start(f32[16,128,128]{2,1,0:T(8,128)} %all-gather.12.cloned.1.call-done) | copy-start | bytes 3145732
  139.7 106.4 %all-gather.18.cloned.1.call-start = ((), (), s32[]{:S(2)}) async-start(), calls=%async_computation.6 | async-start | bytes 2359296 | tf_op jit(solution)/shard_map/all_gather | solution.py:25
  162.2 3.5 %copy-start.22 = (f32[16,128,128]{2,1,0:T(8,128)S(1)}, f32[16,128,128]{2,1,0:T(8,128)}, u32[]{:S(2)}) copy-start(f32[16,128,128]{2,1,0:T(8,128)} %all-gather.16.cloned.1.call-done) | copy-start | bytes 3145732
  163.6 4.4 %copy-start.26 = (bf16[2,2,128]{2,1,0:T(2,128)(2,1)S(1)}, bf16[2,2,128]{2,1,0:T(2,128)(2,1)}, u32[]{:S(2)}) copy-start(bf16[2,2,128]{2,1,0:T(2,128)(2,1)} %param.27) | copy-start | bytes 3076
  163.6 4.5 %copy-start.27 = (bf16[2,2,128]{2,1,0:T(2,128)(2,1)S(1)}, bf16[2,2,128]{2,1,0:T(2,128)(2,1)}, u32[]{:S(2)}) copy-start(bf16[2,2,128]{2,1,0:T(2,128)(2,1)} %param.28) | copy-start | bytes 3076
  163.6 4.7 %copy-start.29 = (f32[2,2]{1,0:T(2,128)S(1)}, f32[2,2]{1,0:T(2,128)}, u32[]{:S(2)}) copy-start(f32[2,2]{1,0:T(2,128)} %param.30) | copy-start | bytes 52
  163.6 4.8 %copy-start.32 = (f32[128]{0:T(128)S(1)}, f32[128]{0:T(128)}, u32[]{:S(2)}) copy-start(f32[128]{0:T(128)} %param.26) | copy-start | bytes 1540
  168.4 4.3 %copy-start.8 = (f32[4,128,128]{2,1,0:T(8,128)S(1)}, f32[4,128,128]{2,1,0:T(8,128)}, u32[]{:S(2)}) copy-start(f32[4,128,128]{2,1,0:T(8,128)} %copy-done.7) | copy-start | bytes 786436
  168.4 4.3 %copy-start.10 = (f32[4,128,128]{2,1,0:T(8,128)S(1)}, f32[4,128,128]{2,1,0:T(8,128)}, u32[]{:S(2)}) copy-start(f32[4,128,128]{2,1,0:T(8,128)} %copy-done.9) | copy-start | bytes 786436
  168.4 4.3 %copy-start.12 = (f32[4,128,128]{2,1,0:T(8,128)S(1)}, f32[4,128,128]{2,1,0:T(8,128)}, u32[]{:S(2)}) copy-start(f32[4,128,128]{2,1,0:T(8,128)} %fusion.109) | copy-start | bytes 786436
  168.4 4.3 %copy-start.18 = (f32[4,128,128]{2,1,0:T(8,128)S(1)}, f32[4,128,128]{2,1,0:T(8,128)}, u32[]{:S(2)}) copy-start(f32[4,128,128]{2,1,0:T(8,128)} %copy-done.17) | copy-start | bytes 786436
  246.2 3.0 %copy-start.6 = (f32[32,128,128]{2,1,0:T(8,128)S(1)}, f32[32,128,128]{2,1,0:T(8,128)}, u32[]{:S(2)}) copy-start(f32[32,128,128]{2,1,0:T(8,128)} %all-gather.14.cloned.1.call-done) | copy-start | bytes 6291460
  246.2 4.3 %copy-start.19 = (f32[32,128,128]{2,1,0:T(8,128)S(1)}, f32[32,128,128]{2,1,0:T(8,128)}, u32[]{:S(2)}) copy-start(f32[32,128,128]{2,1,0:T(8,128)} %all-gather.18.cloned.1.call-done) | copy-start | bytes 6291460
  254.7 17.6 %all-to-all-start = ((bf16[32,2,2,4,128]{4,3,2,1,0:T(4,128)(2,1)}), bf16[32,2,2,4,128]{4,3,2,1,0:T(4,128)(2,1)S(1)}, u32[]{:S(2)}, u32[]{:S(2)}) async-start(bf16[32,2,2,4,128]{4,3,2,1,0:T(4,128)(2,1)} %bitcast.193), calls=%async_computation | async-start | bytes 262144 | tf_op jit(solution)/shard_map/all_to_all | solution.py:42
  263.9 24.0 %copy-start.30 = (bf16[2,2,128]{2,1,0:T(2,128)(2,1)S(1)}, bf16[2,2,128]{2,1,0:T(2,128)(2,1)}, u32[]{:S(2)}) copy-start(bf16[2,2,128]{2,1,0:T(2,128)(2,1)} %param.29) | copy-start | bytes 3076
  263.9 24.0 %copy-start.31 = (f32[2,2]{1,0:T(2,128)S(1)}, f32[2,2]{1,0:T(2,128)}, u32[]{:S(2)}) copy-start(f32[2,2]{1,0:T(2,128)} %param.31) | copy-start | bytes 52
  272.4 16.4 %copy-start.25 = (bf16[2,2,4,128]{3,2,1,0:T(4,128)(2,1)}, bf16[2,2,4,128]{3,2,1,0:T(4,128)(2,1)S(1)}, u32[]{:S(2)}) copy-start(bf16[2,2,4,128]{3,2,1,0:T(4,128)(2,1)S(1)} %reduce_sum.87) | copy-start | bytes 12292
  273.4 14.4 %all-to-all-start.1 = ((f32[32,1,1024]{2,1,0:T(1,128)}), f32[32,1,1024]{2,1,0:T(1,128)S(1)}, u32[]{:S(2)}, u32[]{:S(2)}) async-start(f32[32,1,1024]{2,1,0:T(1,128)} %broadcast_in_dim.80), calls=%async_computation.1 | async-start | bytes 262144 | tf_op jit(solution)/shard_map/all_to_all | solution.py:48
  (16 other events, 17.8 us)
Sparse Core Ops, SparseCore 0:
  9.8 32.1 all-gather.9
  105.7 27.5 all-gather.11
  135.1 27.0 all-gather.15
  163.8 41.2 all-gather.13
  206.7 39.4 all-gather.17
where the time goes:
time: 296 us; the launch traced here: 295 us
  waiting for transfers between devices  172 us (58%)
  matrix products  75.5 us (26%)
  between operations  14.6 us (5%)
  local copies, waits for them, and re-layouts  13.8 us (5%)
  starting transfers between devices  11.1 us (4%)
  other arithmetic  8.51 us (3%)
    all_gather x4, waiting for transfers between devices, carried_in(): pieces = jax.tree.map(lambda part: lax.all_gather(part, axis), subtotal)  122 us
    dot_general x61, matrix products, matmul(): return jnp.einsum(form, left, right, precision=highest)  55.6 us
    all_gather x1, waiting for transfers between devices, shards(): lax.all_gather(tokens, 'tp', axis=2, tiled=True)  32.6 us
    dot_general x6, matrix products, project_rows(): jnp.dot(flat_rows, weight, preferred_element_type=jnp.float32)  19.9 us
    all_to_all x1, waiting for transfers between devices, copy_for_each(): lax.all_to_all(jnp.broadcast_to(value[None], (length, *value.shape)), axi...  8.81 us
    all_to_all x1, waiting for transfers between devices, summed_on_arrival(): lax.all_to_all(parts, axis, split_axis=0, concat_axis=0, tiled=True)  7.1 us
    all_to_all x1, starting transfers between devices, summed_on_arrival(): lax.all_to_all(parts, axis, split_axis=0, concat_axis=0, tiled=True)  7.08 us
  transfers between devices with their start and end apart: 7, of which 7 were waited for; matrix products, arithmetic and copies ran while one was open for 7% of the time, Pallas kernels for 0%

commit v1 on v0

--- a/solution.py
+++ b/solution.py
@@ -179,10 +179,19 @@
     new_beta,
     new_decay,
 ):
+
+    def connect_the_types(page):
+        num = lax.psum(1, axis_name="tp")
+        raw_out = range(page.ndim)
+        y_new = map(lambda to_i: num if to_i == 2 else 1, raw_out)
+        slots = list(y_new)
+        u1 = jnp.tile(page, slots)
+        return lax.all_to_all(u1, "tp", concat_axis=2, tiled=True, split_axis=2)
+
     seq_count, span_len, _ = tokens.shape
     head_count = rate_log.shape[0]
     weights = (query_weight, key_weight, value_weight, gate_weight, beta_weight, decay_weight)
-    totals = project_rows(lax.all_gather(tokens, "tp", axis=2, tiled=True), weights)
+    totals = project_rows(connect_the_types(tokens), weights)
     query_rows = stored(totals[0])
     key_rows = stored(totals[1])
     value_rows = stored(totals[2])

time: 296 us -> 334 us (1.13)
  local copies, waits for them, and re-layouts: 13.8 us -> 28.9 us
  waiting for transfers between devices: 172 us -> 186 us
  starting transfers between devices: 11.1 us -> 17.8 us
    all_to_all x0 -> x1, waiting for transfers between devices: none -> 48.2 us  [connect_the_types(): return lax.all_to_all(u1, 'tp', concat_axis=2, tiled=True, split_axis=2)]
    all_gather x1 -> x0, waiting for transfers between devices: 32.6 us -> none  [shards(): lax.all_gather(tokens, 'tp', axis=2, tiled=True)]
    all_to_all x0 -> x1, local copies, waits for them, and re-layouts: none -> 11 us  [connect_the_types(): return lax.all_to_all(u1, 'tp', concat_axis=2, tiled=True, split_axis=2)]
    all_to_all x0 -> x1, starting transfers between devices: none -> 6.74 us  [connect_the_types(): return lax.all_to_all(u1, 'tp', concat_axis=2, tiled=True, split_axis=2)]
    another operation x0 -> x1, local copies, waits for them, and re-layouts: none -> 4.18 us  [connect_the_types(): u1 = jnp.tile(page, slots)]
    unnamed x68 -> x71, local copies, waits for them, and re-layouts: 5.89 us -> 6.79 us
  transfers between devices with their start and end apart: 7 -> 7, of which waited for: 7 -> 7; matrix products, arithmetic and copies ran while one was open for 7% -> 6% of each run, Pallas kernels for 0% -> 0%
where the time goes in v1:
time: 334 us; the launch traced here: 333 us
  waiting for transfers between devices  186 us (56%)
  matrix products  78.5 us (24%)
  local copies, waits for them, and re-layouts  28.9 us (9%)
  starting transfers between devices  17.8 us (5%)
  between operations  14.6 us (4%)
  other arithmetic  7.13 us (2%)
    all_gather x4, waiting for transfers between devices, carried_in(): pieces = jax.tree.map(lambda part: lax.all_gather(part, axis), subtotal)  121 us
    dot_general x61, matrix products, matmul(): return jnp.einsum(form, left, right, precision=highest)  58.6 us
    all_to_all x1, waiting for transfers between devices, connect_the_types(): return lax.all_to_all(u1, 'tp', concat_axis=2, tiled=True, split_axis=2)  48.2 us
    dot_general x6, matrix products, project_rows(): jnp.dot(flat_rows, weight, preferred_element_type=jnp.float32)  19.9 us
    all_to_all x1, local copies, waits for them, and re-layouts, connect_the_types(): return lax.all_to_all(u1, 'tp', concat_axis=2, tiled=True, split_axis=2)  11 us
    all_to_all x1, waiting for transfers between devices, copy_for_each(): lax.all_to_all(jnp.broadcast_to(value[None], (length, *value.shape)), axi...  8.81 us
    all_to_all x1, waiting for transfers between devices, summed_on_arrival(): lax.all_to_all(parts, axis, split_axis=0, concat_axis=0, tiled=True)  7.1 us
    all_to_all x1, starting transfers between devices, summed_on_arrival(): lax.all_to_all(parts, axis, split_axis=0, concat_axis=0, tiled=True)  7.08 us
  transfers between devices with their start and end apart: 7, of which 7 were waited for; matrix products, arithmetic and copies ran while one was open for 6% of the time, Pallas kernels for 0%

profile of v1, /device:TPU:8, one launch (start us, length us, event | category | flops | bytes accessed | tf_op | source)
XLA Modules:
  0.0 332.8 jit_solution(17022759519218053495)
XLA Ops:
  8.7 4.2 %tile.4 = bf16[2,192,8,512]{1,0,3,2:T(2,128)(2,1)} broadcast(bf16[2,192,512]{1,0,2:T(2,128)(2,1)S(1)} %copy.183), dimensions={0,1,3} | broadcast | bytes 3538944 | tf_op jit(solution)/shard_map/tile | solution.py:188
  12.8 6.7 %all-to-all-start = ((bf16[2,192,4096]{1,0,2:T(2,128)(2,1)}), bf16[2,192,4096]{1,0,2:T(2,128)(2,1)}, u32[]{:S(2)}, u32[]{:S(2)}) async-start(bf16[2,192,4096]{1,0,2:T(2,128)(2,1)} %bitcast.240), calls=%async_computation | async-start | bytes 8388608 | tf_op jit(solution)/shard_map/all_to_all | solution.py:189
  19.7 48.2 %all-to-all-done = bf16[2,192,4096]{1,0,2:T(2,128)(2,1)} async-done(((bf16[2,192,4096]{1,0,2:T(2,128)(2,1)}), bf16[2,192,4096]{1,0,2:T(2,128)(2,1)}, u32[]{:S(2)}, u32[]{:S(2)}) %all-to-all-start) | async-done | bytes 3145760 | tf_op jit(solution)/shard_map/all_to_all | solution.py:189
  67.9 11.0 %copy.184 = bf16[2,192,4096]{2,1,0:T(8,128)(2,1)} copy(bf16[2,192,4096]{1,0,2:T(2,128)(2,1)} %all-to-all-done) | data formatting | bytes 6291456 | tf_op jit(solution)/shard_map/all_to_all | solution.py:189
  78.9 2.8 fusion.91
  83.3 2.9 convolution_convert_fusion.1
  87.1 2.8 fusion.50
  90.0 3.5 %convolution_convert_fusion.3 = bf16[384,256]{1,0:T(8,128)(2,1)S(1)} fusion(bf16[384,4096]{1,0:T(8,128)(2,1)} %bitcast.237, bf16[4096,256]{1,0:T(8,128)(2,1)} %param.19), kind=kOutput, calls=%fused_computation.61 | convolution fusion | flops 805404672 | bytes 5439488 | tf_op jit(solution)/shard_map/dot_general | solution.py:161
  95.1 3.6 %convolution_convert_fusion.2 = bf16[384,256]{1,0:T(8,128)(2,1)S(1)} fusion(bf16[384,4096]{1,0:T(8,128)(2,1)} %bitcast.238, bf16[4096,256]{1,0:T(8,128)(2,1)} %param.20), kind=kOutput, calls=%fused_computation.60 | convolution fusion | flops 805404672 | bytes 5439488 | tf_op jit(solution)/shard_map/dot_general | solution.py:161
  112.6 30.4 %while.17 = (s32[]{:T(128)}, f32[4,128,128]{2,1,0:T(8,128)S(1)}, f32[4,128,128]{2,1,0:T(8,128)S(1)}, f32[3,4,64,128]{3,2,0,1:T(8,128)}, f32[3,4,64,128]{3,2,0,1:...) while((s32[]{:T(128)}, f32[4,128,128]{2,1,0:T(8,128)S(1)}, ...), condition=%wide.region_4.5_spmd.clone, body=%wide.region_3.4_spmd.clone.sunk | while | flops 403210240 | bytes 5445847 | solution.py:232
  115.1 1.9 fusion.227
  125.2 1.9 fusion.227
  135.3 1.9 fusion.227
  144.5 26.1 %all-gather.9.cloned.1.call-done = f32[16,128,128]{2,1,0:T(8,128)} async-done(((f32[4,128,128]{2,1,0:T(8,128)}), f32[16,128,128]{2,1,0:T(8,128)}) %all-gather.9.cloned.1.call-update) | async-done | bytes 1048592 | tf_op jit(solution)/shard_map/all_gather | solution.py:25
  177.1 22.4 %all-gather.13.cloned.1.call-done = f32[16,128,128]{2,1,0:T(8,128)} async-done(((f32[4,128,128]{2,1,0:T(8,128)}), f32[16,128,128]{2,1,0:T(8,128)}) %all-gather.13.cloned.1.call-update) | async-done | bytes 1048592 | tf_op jit(solution)/shard_map/all_gather | solution.py:25
  205.8 4.3 %convolution_convert_fusion = bf16[384,256]{1,0:T(8,128)(2,1)} fusion(bf16[384,4096]{1,0:T(8,128)(2,1)} %bitcast.239, bf16[4096,256]{1,0:T(8,128)(2,1)} %param.21), kind=kOutput, calls=%fused_computation.58 | convolution fusion | flops 805404672 | bytes 5439488 | tf_op jit(solution)/shard_map/dot_general | solution.py:161
  211.2 31.3 %all-gather.11.cloned.1.call-done = f32[32,128,128]{2,1,0:T(8,128)} async-done(((f32[4,128,128]{2,1,0:T(8,128)}), f32[32,128,128]{2,1,0:T(8,128)}) %all-gather.11.cloned.1.call-update) | async-done | bytes 2097168 | tf_op jit(solution)/shard_map/all_gather | solution.py:25
  242.5 41.1 %all-gather.15.cloned.1.call-done = f32[32,128,128]{2,1,0:T(8,128)} async-done(((f32[4,128,128]{2,1,0:T(8,128)}), f32[32,128,128]{2,1,0:T(8,128)}) %all-gather.15.cloned.1.call-update) | async-done | bytes 2097168 | tf_op jit(solution)/shard_map/all_gather | solution.py:25
  292.2 7.1 %all-to-all-start.1 = ((bf16[32,2,2,4,128]{4,3,2,1,0:T(4,128)(2,1)}), bf16[32,2,2,4,128]{4,3,2,1,0:T(4,128)(2,1)S(1)}, u32[]{:S(2)}, u32[]{:S(2)}) async-start(bf16[32,2,2,4,128]{4,3,2,1,0:T(4,128)(2,1)} %bitcast.194), calls=%async_computation.1 | async-start | bytes 262144 | tf_op jit(solution)/shard_map/all_to_all | solution.py:42
  299.3 1.6 fusion.38
  302.7 7.1 %all-to-all-done.1 = bf16[32,2,2,4,128]{4,3,2,1,0:T(4,128)(2,1)S(1)} async-done(((bf16[32,2,2,4,128]{4,3,2,1,0:T(4,128)(2,1)}), bf16[32,2,2,4,128]{4,3,2,1,0:T(4,128)(2,1)S(1)}, u32[]{:S(2)}, u32[]{:S(2)}) %all-to-all-start.1) | async-done | bytes 131104 | tf_op jit(solution)/shard_map/all_to_all | solution.py:42
  310.9 3.8 %all-to-all-start.2 = ((f32[32,1,1024]{2,1,0:T(1,128)}), f32[32,1,1024]{2,1,0:T(1,128)S(1)}, u32[]{:S(2)}, u32[]{:S(2)}) async-start(f32[32,1,1024]{2,1,0:T(1,128)} %broadcast_in_dim.80), calls=%async_computation.2 | async-start | bytes 262144 | tf_op jit(solution)/shard_map/all_to_all | solution.py:48
  314.7 1.7 fusion.60
  316.5 8.8 %all-to-all-done.2 = f32[32,1,1024]{2,1,0:T(1,128)S(1)} async-done(((f32[32,1,1024]{2,1,0:T(1,128)}), f32[32,1,1024]{2,1,0:T(1,128)S(1)}, u32[]{:S(2)}, u32[]{:S(2)}) %all-to-all-start.2) | async-done | bytes 131104 | tf_op jit(solution)/shard_map/all_to_all | solution.py:48
  (199 shorter events, 71.2 us)
Async XLA Ops:
  7.2 76.1 %copy-start = (bf16[4096,256]{1,0:T(8,128)(2,1)S(1)}, bf16[4096,256]{1,0:T(8,128)(2,1)}, u32[]{:S(2)}) copy-start(bf16[4096,256]{1,0:T(8,128)(2,1)} %param.18) | copy-start | bytes 6291460
  12.8 6.8 %copy-start.33 = (f32[2]{0:T(128)S(1)}, f32[2]{0:T(128)}, u32[]{:S(2)}) copy-start(f32[2]{0:T(128)} %param.25) | copy-start | bytes 28
  12.8 55.1 %all-to-all-start = ((bf16[2,192,4096]{1,0,2:T(2,128)(2,1)}), bf16[2,192,4096]{1,0,2:T(2,128)(2,1)}, u32[]{:S(2)}, u32[]{:S(2)}) async-start(bf16[2,192,4096]{1,0,2:T(2,128)(2,1)} %bitcast.240), calls=%async_computation | async-start | bytes 8388608 | tf_op jit(solution)/shard_map/all_to_all | solution.py:189
  19.6 151.0 %all-gather.9.cloned.1.call-start = ((), (), s32[]{:S(2)}) async-start(), calls=%async_computation.3 | async-start | bytes 1310720 | tf_op jit(solution)/shard_map/all_gather | solution.py:25
  19.7 59.2 %copy-start.23 = (bf16[4096,2]{0,1:T(2,128)(2,1)S(1)}, bf16[4096,2]{0,1:T(2,128)(2,1)}, u32[]{:S(2)}) copy-start(bf16[4096,2]{0,1:T(2,128)(2,1)} %param.23) | copy-start | bytes 49156
  95.1 5.6 %copy-start.20 = (f32[2,2,3,64,128]{4,3,1,0,2:T(8,128)S(1)}, f32[2,2,3,64,128]{4,3,1,0,2:T(8,128)}, u32[]{:S(2)}) copy-start(f32[2,2,3,64,128]{4,3,1,0,2:T(8,128)} %copy.187) | copy-start | bytes 1179652
  143.7 55.8 %all-gather.13.cloned.1.call-start = ((), (), s32[]{:S(2)}) async-start(), calls=%async_computation.5 | async-start | bytes 1310720 | tf_op jit(solution)/shard_map/all_gather | solution.py:25
  144.4 98.1 %all-gather.11.cloned.1.call-start = ((), (), s32[]{:S(2)}) async-start(), calls=%async_computation.4 | async-start | bytes 2359296 | tf_op jit(solution)/shard_map/all_gather | solution.py:25
  170.6 4.2 %copy-start.3 = (f32[16,128,128]{2,1,0:T(8,128)S(1)}, f32[16,128,128]{2,1,0:T(8,128)}, u32[]{:S(2)}) copy-start(f32[16,128,128]{2,1,0:T(8,128)} %all-gather.9.cloned.1.call-done) | copy-start | bytes 3145732
  177.1 106.6 %all-gather.15.cloned.1.call-start = ((), (), s32[]{:S(2)}) async-start(), calls=%async_computation.6 | async-start | bytes 2359296 | tf_op jit(solution)/shard_map/all_gather | solution.py:25
  200.9 4.4 %copy-start.26 = (bf16[2,2,128]{2,1,0:T(2,128)(2,1)S(1)}, bf16[2,2,128]{2,1,0:T(2,128)(2,1)}, u32[]{:S(2)}) copy-start(bf16[2,2,128]{2,1,0:T(2,128)(2,1)} %param.27) | copy-start | bytes 3076
  200.9 4.5 %copy-start.27 = (bf16[2,2,128]{2,1,0:T(2,128)(2,1)S(1)}, bf16[2,2,128]{2,1,0:T(2,128)(2,1)}, u32[]{:S(2)}) copy-start(bf16[2,2,128]{2,1,0:T(2,128)(2,1)} %param.28) | copy-start | bytes 3076
  200.9 4.8 %copy-start.29 = (f32[2,2]{1,0:T(2,128)S(1)}, f32[2,2]{1,0:T(2,128)}, u32[]{:S(2)}) copy-start(f32[2,2]{1,0:T(2,128)} %param.30) | copy-start | bytes 52
  200.9 4.8 %copy-start.32 = (f32[128]{0:T(128)S(1)}, f32[128]{0:T(128)}, u32[]{:S(2)}) copy-start(f32[128]{0:T(128)} %param.26) | copy-start | bytes 1540
  205.7 4.3 %copy-start.8 = (f32[4,128,128]{2,1,0:T(8,128)S(1)}, f32[4,128,128]{2,1,0:T(8,128)}, u32[]{:S(2)}) copy-start(f32[4,128,128]{2,1,0:T(8,128)} %copy-done.7) | copy-start | bytes 786436
  205.8 4.3 %copy-start.10 = (f32[4,128,128]{2,1,0:T(8,128)S(1)}, f32[4,128,128]{2,1,0:T(8,128)}, u32[]{:S(2)}) copy-start(f32[4,128,128]{2,1,0:T(8,128)} %copy-done.9) | copy-start | bytes 786436
  205.8 4.3 %copy-start.12 = (f32[4,128,128]{2,1,0:T(8,128)S(1)}, f32[4,128,128]{2,1,0:T(8,128)}, u32[]{:S(2)}) copy-start(f32[4,128,128]{2,1,0:T(8,128)} %fusion.109) | copy-start | bytes 786436
  205.8 4.3 %copy-start.18 = (f32[4,128,128]{2,1,0:T(8,128)S(1)}, f32[4,128,128]{2,1,0:T(8,128)}, u32[]{:S(2)}) copy-start(f32[4,128,128]{2,1,0:T(8,128)} %copy-done.17) | copy-start | bytes 786436
  283.6 4.3 %copy-start.19 = (f32[32,128,128]{2,1,0:T(8,128)S(1)}, f32[32,128,128]{2,1,0:T(8,128)}, u32[]{:S(2)}) copy-start(f32[32,128,128]{2,1,0:T(8,128)} %all-gather.15.cloned.1.call-done) | copy-start | bytes 6291460
  292.2 17.6 %all-to-all-start.1 = ((bf16[32,2,2,4,128]{4,3,2,1,0:T(4,128)(2,1)}), bf16[32,2,2,4,128]{4,3,2,1,0:T(4,128)(2,1)S(1)}, u32[]{:S(2)}, u32[]{:S(2)}) async-start(bf16[32,2,2,4,128]{4,3,2,1,0:T(4,128)(2,1)} %bitcast.194), calls=%async_computation.1 | async-start | bytes 262144 | tf_op jit(solution)/shard_map/all_to_all | solution.py:42
  301.4 24.0 %copy-start.30 = (bf16[2,2,128]{2,1,0:T(2,128)(2,1)S(1)}, bf16[2,2,128]{2,1,0:T(2,128)(2,1)}, u32[]{:S(2)}) copy-start(bf16[2,2,128]{2,1,0:T(2,128)(2,1)} %param.29) | copy-start | bytes 3076
  301.4 24.0 %copy-start.31 = (f32[2,2]{1,0:T(2,128)S(1)}, f32[2,2]{1,0:T(2,128)}, u32[]{:S(2)}) copy-start(f32[2,2]{1,0:T(2,128)} %param.31) | copy-start | bytes 52
  309.9 16.4 %copy-start.25 = (bf16[2,2,4,128]{3,2,1,0:T(4,128)(2,1)}, bf16[2,2,4,128]{3,2,1,0:T(4,128)(2,1)S(1)}, u32[]{:S(2)}) copy-start(bf16[2,2,4,128]{3,2,1,0:T(4,128)(2,1)S(1)} %reduce_sum.87) | copy-start | bytes 12292
  310.9 14.4 %all-to-all-start.2 = ((f32[32,1,1024]{2,1,0:T(1,128)}), f32[32,1,1024]{2,1,0:T(1,128)S(1)}, u32[]{:S(2)}, u32[]{:S(2)}) async-start(f32[32,1,1024]{2,1,0:T(1,128)} %broadcast_in_dim.80), calls=%async_computation.2 | async-start | bytes 262144 | tf_op jit(solution)/shard_map/all_to_all | solution.py:48
  (17 other events, 20.4 us)
Sparse Core Ops, SparseCore 0:
  143.8 26.7 all-gather.8
  172.4 27.0 all-gather.12
  201.3 41.2 all-gather.10
  244.2 39.4 all-gather.14
